TPU v7x, 32 devices: a whole 2x2x4 slice. The times are simulated.
32 devices in a mesh: ep: 8 (over z, core), tp: 4 (over y, x).
Axes of the slice: x: 2, y: 2, z: 4, core: 2. Of those that a mesh axis runs over, the one named last changes fastest.
Arguments:
- tokens: bfloat16 [128, 2048], P('ep'), may hold values from -6 to 6
- old_state: float32 [128, 16, 128, 128], P('ep', 'tp'), may hold values from -2 to 2
- lower_bound: float32 [2048], P('tp'), may hold values from 0.05 to 0.95
- head_gain: float32 [2048], P('tp'), may hold values from 0.1 to 1.9
- norm_gains: float32 [4, 2048], replicated, may hold values from 0.1 to 1.9
- w_query: bfloat16 [2048, 2048], P('ep', 'tp'), may hold values from -0.125 to 0.125
- w_forget: bfloat16 [2048, 2048], P('ep', 'tp'), may hold values from -0.125 to 0.125
- w_value: bfloat16 [2048, 2048], P('ep', 'tp'), may hold values from -0.125 to 0.125
- w_outgate: bfloat16 [2048, 2048], P('ep', 'tp'), may hold values from -0.125 to 0.125
- w_mix_out: bfloat16 [2048, 2048], P('tp', 'ep'), may hold values from -0.125 to 0.125
- routes: int32 [128, 2], P('ep'), may hold values from 0 to 7, all different within a row; in each aligned block of 16 rows (0 to 15, 16 to 31, ...) at most 8 rows name the same one
- route_scores: float32 [128, 2], P('ep'), may hold values from -6 to 6
- w_exp_gate: bfloat16 [8, 2048, 3584], P('ep', None, 'tp'), may hold values from -0.125 to 0.125
- w_exp_up: bfloat16 [8, 2048, 3584], P('ep', None, 'tp'), may hold values from -0.125 to 0.125
- w_exp_down: bfloat16 [8, 3584, 2048], P('ep', 'tp'), may hold values from -0.75 to 0.75
- w_dense_gate: bfloat16 [2048, 6144], P('ep', 'tp'), may hold values from -0.125 to 0.125
- w_dense_up: bfloat16 [2048, 6144], P('ep', 'tp'), may hold values from -0.125 to 0.125
- w_dense_down: bfloat16 [6144, 2048], P('tp', 'ep'), may hold values from -0.75 to 0.75
- dense_mix: bfloat16 [2048], replicated, may hold values from -0.125 to 0.125
Outputs:
- layer_out: bfloat16 [128, 2048], P('ep', 'tp')
- new_state: float32 [128, 16, 128, 128], P('ep', 'tp')
Inputs may be any that keep to these rules, and one draw needn't show every extreme that they name: `routes`: each row names 2 different experts. In each aligned block of 16 rows no expert is named by more than 8 rows, and in every draw some expert is named by exactly 8 rows of some block.
All inputs are finite; a program needn't handle non-finite values.
Results may differ from a plain program's by a relative error of at most 0.025.
Values may be sent and summed in bfloat16 or wider, within the bound.
No kernel may reach another device: no remote copies, remote signals or barrier semaphores. Data moves between devices by JAX's collectives and lax.ppermute only.
A program may use at most 64 MiB of HBM per device.

v0:
```python
import jax
import jax.numpy as jnp
from jax import lax
from jax.sharding import PartitionSpec as P

EPS = 1e-06


def rms_scale(values):
    return lax.rsqrt(jnp.mean(values * values, axis=-1, keepdims=True) + EPS)


def body(
    tokens,
    old_state,
    lower_bound,
    head_gain,
    norm_gains,
    w_query,
    w_forget,
    w_value,
    w_outgate,
    w_mix_out,
    routes,
    route_scores,
    w_exp_gate,
    w_exp_up,
    w_exp_down,
    w_dense_gate,
    w_dense_up,
    w_dense_down,
    dense_mix,
):
    highest = lax.Precision.HIGHEST
    seqs, width = tokens.shape
    column_index = lax.axis_index("tp")
    part_width = width // lax.axis_size("tp")
    resid = tokens.astype(jnp.float32)
    normed = (resid * rms_scale(resid) * norm_gains[0]).astype(jnp.bfloat16)
    in_weights = jnp.concatenate([w_query, w_forget, w_value, w_outgate], axis=1)
    mix_rows = lax.all_to_all(normed, "ep", split_axis=1, concat_axis=0, tiled=True)
    projected = lax.psum_scatter(
        jnp.dot(mix_rows, in_weights, preferred_element_type=jnp.float32).astype(jnp.bfloat16),
        "ep",
        scatter_dimension=0,
        tiled=True,
    ).astype(jnp.float32)
    query_raw, forget_raw, value, out_gate = jnp.split(projected, 4, axis=1)
    heads = old_state.shape[1]
    head_size = old_state.shape[2]
    shape_heads = (seqs, heads, head_size)
    forget = lower_bound + (1.0 - lower_bound) * jax.nn.sigmoid(forget_raw)
    key_in = (1.0 - lower_bound) * jax.nn.sigmoid(-forget_raw)
    new_state = forget.reshape(shape_heads)[..., None] * old_state + key_in.reshape(shape_heads)[
        ..., None
    ] * value.reshape(seqs, heads, 1, head_size)
    query = jax.nn.silu(query_raw).reshape(shape_heads)
    read = jnp.einsum("thk,thkv->thv", query, new_state, precision=highest)
    gated = (
        read
        * rms_scale(read)
        * head_gain.reshape(heads, head_size)
        * jax.nn.silu(out_gate).reshape(shape_heads)
    )
    mixed_heads = gated.reshape(seqs, heads * head_size).astype(jnp.bfloat16)
    mix_part = jnp.dot(
        mixed_heads,
        lax.all_gather(w_mix_out, "ep", axis=1, tiled=True),
        preferred_element_type=jnp.float32,
    ).astype(jnp.bfloat16)
    mix_part = lax.optimization_barrier(mix_part).astype(jnp.float32)
    mix_out = lax.psum(mix_part.astype(jnp.bfloat16), "tp")
    mix_wide = lax.optimization_barrier(mix_out).astype(jnp.float32)
    after_mix = resid + mix_wide * rms_scale(mix_wide) * norm_gains[1]
    ffn_in = (after_mix * rms_scale(after_mix) * norm_gains[2]).astype(jnp.bfloat16)
    experts = lax.axis_size("ep")
    topk = routes.shape[1]
    capacity = max(2, 2 * seqs * topk // experts)
    flat_routes = routes.reshape(-1)
    onehot = (flat_routes[:, None] == jnp.arange(experts, dtype=jnp.int32)[None, :]).astype(
        jnp.int32
    )
    before = jnp.cumsum(onehot, axis=0) - onehot
    slots = jnp.sum(onehot * before, axis=1)
    cells = flat_routes * capacity + slots
    placed = cells[None, :] == jnp.arange(experts * capacity, dtype=jnp.int32)[:, None]
    repeated = jnp.repeat(ffn_in, topk, axis=0)
    outgoing = jnp.dot(placed.astype(jnp.bfloat16), repeated, preferred_element_type=jnp.float32)
    outgoing = outgoing.astype(jnp.bfloat16).reshape(experts, capacity, width)
    arrived = lax.all_to_all(outgoing, "ep", split_axis=0, concat_axis=0, tiled=True)
    sources, items, _ = arrived.shape
    expert_rows = arrived.reshape(sources * items, width)
    gate_pre = jnp.dot(expert_rows, w_exp_gate[0], preferred_element_type=jnp.float32)
    up_pre = jnp.dot(expert_rows, w_exp_up[0], preferred_element_type=jnp.float32)
    hidden = (jax.nn.silu(gate_pre) * up_pre).astype(jnp.bfloat16)
    partial_rows = jnp.dot(hidden, w_exp_down[0], preferred_element_type=jnp.float32).astype(
        jnp.bfloat16
    )
    partial_rows = lax.optimization_barrier(partial_rows).astype(jnp.float32)
    partial_rows = partial_rows.reshape(sources, items, width)
    summed = lax.psum_scatter(
        partial_rows.astype(jnp.bfloat16), "tp", scatter_dimension=2, tiled=True
    )
    returned = lax.all_to_all(summed, "ep", split_axis=0, concat_axis=0, tiled=True)
    first = jax.nn.sigmoid(route_scores[:, 0] - route_scores[:, 1])
    second = jax.nn.sigmoid(route_scores[:, 1] - route_scores[:, 0])
    route_weight = jnp.stack([first, second], axis=1).reshape(-1)
    weight_table = jnp.sum(
        (placed.astype(jnp.float32) * route_weight[None, :]).reshape(
            experts * capacity, seqs, topk
        ),
        axis=2,
    )
    expert_sum = jnp.dot(
        weight_table.T,
        returned.reshape(experts * capacity, part_width).astype(jnp.float32),
        precision=highest,
    )
    dense_weights = jnp.concatenate([w_dense_gate, w_dense_up], axis=1)
    dense_rows = lax.all_to_all(ffn_in, "ep", split_axis=1, concat_axis=0, tiled=True)
    dense_pre = lax.psum_scatter(
        jnp.dot(dense_rows, dense_weights, preferred_element_type=jnp.float32).astype(jnp.bfloat16),
        "ep",
        scatter_dimension=0,
        tiled=True,
    ).astype(jnp.float32)
    dense_gate_pre, dense_up_pre = jnp.split(dense_pre, 2, axis=1)
    dense_hidden = (jax.nn.silu(dense_gate_pre) * dense_up_pre).astype(jnp.bfloat16)
    dense_partial = jnp.dot(
        dense_hidden,
        lax.all_gather(w_dense_down, "ep", axis=1, tiled=True),
        preferred_element_type=jnp.float32,
    )
    dense_out = lax.psum_scatter(
        dense_partial.astype(jnp.bfloat16), "tp", scatter_dimension=1, tiled=True
    ).astype(jnp.float32)
    mix_weight = jax.nn.sigmoid(jnp.dot(ffn_in, dense_mix, preferred_element_type=jnp.float32))
    ffn_out = expert_sum + mix_weight[:, None] * dense_out
    squares = lax.psum(jnp.sum(ffn_out * ffn_out, axis=1), "tp")
    out_scale = lax.rsqrt(squares / width + EPS)
    gain_part = lax.dynamic_slice_in_dim(norm_gains[3], column_index * part_width, part_width, 0)
    resid_part = lax.dynamic_slice_in_dim(after_mix, column_index * part_width, part_width, 1)
    layer_out = (resid_part + ffn_out * out_scale[:, None] * gain_part).astype(jnp.bfloat16)
    return (layer_out, new_state)


def solution(mesh):
    return jax.shard_map(
        body,
        mesh=mesh,
        in_specs=(
            P("ep", None),
            P("ep", "tp", None, None),
            P("tp"),
            P("tp"),
            P(),
            P("ep", "tp"),
            P("ep", "tp"),
            P("ep", "tp"),
            P("ep", "tp"),
            P("tp", "ep"),
            P("ep", None),
            P("ep", None),
            P("ep", None, "tp"),
            P("ep", None, "tp"),
            P("ep", "tp", None),
            P("ep", "tp"),
            P("ep", "tp"),
            P("tp", "ep"),
            P(),
        ),
        out_specs=(P("ep", "tp"), P("ep", "tp", None, None)),
        check_vma=False,
    )
```

profile of v0, /device:TPU:0, one launch (start us, length us, event | category | flops | bytes accessed | tf_op | source)
XLA Modules:
  0.0 319.4 jit_solution(3477213161517081613)
XLA Ops:
  7.2 0.9 fusion.58
  8.2 1.0 fusion.42
  9.2 0.9 fusion.44
  10.1 12.1 %all_to_all.48 = bf16[16,8,256]{2,0,1:T(8,128)(2,1)S(1)} all-to-all(bf16[16,8,256]{2,0,1:T(8,128)(2,1)S(1)} %bitcast.82), channel_id=1, replica_groups=mesh['ep'=8,'tp'=4] {'ep'}, dimensions={1} | all-to-all | bytes 131072 | tf_op jit(solution)/shard_map/all_to_all | solution.py:41
  22.2 2.3 convolution_convert_fusion.1
  24.5 0.7 all-gather.3.cloned.1.call-update
  25.8 28.7 %reduce-scatter.5.cloned.1.call-done = bf16[16,2048]{1,0:T(8,128)(2,1)} async-done(((bf16[128,2048]{1,0:T(8,128)(2,1)}), bf16[16,2048]{1,0:T(8,128)(2,1)}) %reduce-scatter.5.cloned.1.call-update) | async-done | bytes 65552 | tf_op jit(solution)/shard_map/reduce_scatter | solution.py:42
  54.5 0.8 convert_element_type.70
  55.4 0.7 split.26
  56.2 4.4 %multiply_add_fusion = f32[16,4,128,128]{3,2,1,0:T(8,128)S(1)} fusion(f32[16,4,128,128]{3,2,1,0:T(8,128)} %param.20, f32[16,4,128]{2,1,0:T(4,128)S(1)} %mul.223, f32[16,4,128]{2,1,0:T(4,128)S(1)} %mul.221, f32[16,4,128]{2,1,0:T(4,128)S(1)} %mul.217), kind=kLoop, calls=%fused_computation | loop fusion | flops 3145728 | bytes 8486912 | tf_op jit(solution)/shard_map/add | solution.py:54
  60.7 2.0 copy-done
  62.6 3.7 %fusion.59 = f32[16,4,1,128]{3,2,1,0:T(1,128)S(1)} fusion(f32[16,4,128,1]{2,3,1,0:T(1,128)S(1)} %bitcast.84, f32[16,4,128,128]{3,2,1,0:T(8,128)S(1)} %multiply_add_fusion), kind=kOutput, calls=%fused_computation.92 | convolution fusion | flops 12582912 | bytes 4259840 | tf_op jit(solution)/shard_map/thk,thkv->thv/dot_general | solution.py:58
  66.5 18.5 %all-gather.3.cloned.1.call-done = bf16[512,2048]{1,0:T(8,128)(2,1)} async-done(((bf16[512,256]{1,0:T(8,128)(2,1)}), bf16[512,2048]{1,0:T(8,128)(2,1)}) %all-gather.3.cloned.1.call-update) | async-done | bytes 2097168 | tf_op jit(solution)/shard_map/all_gather | solution.py:68
  85.0 2.6 convolution_convert_fusion.4
  87.7 41.1 %all-reduce.2.cloned.1.call-done = bf16[16,2048]{1,0:T(8,128)(2,1)} async-done(((bf16[16,2048]{1,0:T(8,128)(2,1)}), bf16[16,2048]{1,0:T(8,128)(2,1)}) %all-reduce.2.cloned.1.call-update) | async-done | bytes 65552 | tf_op jit(solution)/shard_map/psum | solution.py:72
  128.8 1.0 fusion.40
  129.7 1.0 multiply_reduce_fusion
  131.2 14.1 %all_to_all.49 = bf16[8,8,2048]{2,1,0:T(8,128)(2,1)S(1)} all-to-all(bf16[8,8,2048]{2,1,0:T(8,128)(2,1)S(1)} %fusion.9), channel_id=1, replica_groups=mesh['ep'=8,'tp'=4] {'ep'}, dimensions={0} | all-to-all | bytes 524288 | tf_op jit(solution)/shard_map/all_to_all | solution.py:90
  145.4 2.7 fusion.4
  148.1 5.5 %fusion.6 = bf16[64,2048]{1,0:T(8,128)(2,1)} fusion(bf16[1,896,2048]{2,1,0:T(8,128)(2,1)} %param.33, bf16[1,2048,896]{2,1,0:T(8,128)(2,1)} %param.32, bf16[8,8,2048]{2,1,0:T(8,128)(2,1)S(1)} %all_to_all.49, f32[64,896]{1,0:T(8,128)S(1)} %fusion.4), kind=kOutput, calls=%fused_computation.9 | convolution fusion | flops 470237184 | bytes 8093696 | tf_op jit(solution)/shard_map/dot_general | solution.py:96
  153.7 8.3 %all_to_all.50 = bf16[16,8,256]{2,0,1:T(8,128)(2,1)S(1)} all-to-all(bf16[16,8,256]{2,0,1:T(8,128)(2,1)S(1)} %bitcast.83), channel_id=1, replica_groups=mesh['ep'=8,'tp'=4] {'ep'}, dimensions={1} | all-to-all | bytes 131072 | tf_op jit(solution)/shard_map/all_to_all | solution.py:120
  162.0 1.3 convolution_convert_fusion
  164.2 11.9 %reduce-scatter.7.cloned.1.call-done = bf16[8,8,512]{2,1,0:T(8,128)(2,1)} async-done(((bf16[8,8,2048]{2,1,0:T(8,128)(2,1)}), bf16[8,8,512]{2,1,0:T(8,128)(2,1)}) %reduce-scatter.7.cloned.1.call-update) | async-done | bytes 65552 | tf_op jit(solution)/shard_map/reduce_scatter | solution.py:101
  176.1 4.6 %all-to-all-start.2 = ((bf16[8,8,512]{2,1,0:T(8,128)(2,1)}), bf16[8,8,512]{2,1,0:T(8,128)(2,1)S(1)}, u32[]{:S(2)}, u32[]{:S(2)}) async-start(bf16[8,8,512]{2,1,0:T(8,128)(2,1)} %reduce-scatter.7.cloned.1.call-done), calls=%async_computation.4 | async-start | bytes 131072 | tf_op jit(solution)/shard_map/all_to_all | solution.py:104
  180.8 29.5 %reduce-scatter.9.cloned.1.call-done = bf16[16,3072]{1,0:T(8,128)(2,1)} async-done(((bf16[128,3072]{1,0:T(8,128)(2,1)}), bf16[16,3072]{1,0:T(8,128)(2,1)}) %reduce-scatter.9.cloned.1.call-update) | async-done | bytes 98320 | tf_op jit(solution)/shard_map/reduce_scatter | solution.py:121
  210.3 0.9 convert_element_type.82
  211.2 63.9 %all-gather.5.cloned.1.call-done = bf16[1536,2048]{1,0:T(8,128)(2,1)} async-done(((bf16[1536,256]{1,0:T(8,128)(2,1)}), bf16[1536,2048]{1,0:T(8,128)(2,1)}) %all-gather.5.cloned.1.call-update) | async-done | bytes 6291472 | tf_op jit(solution)/shard_map/all_gather | solution.py:131
  275.1 4.3 %convolution_convert_fusion.3 = bf16[16,2048]{1,0:T(8,128)(2,1)} fusion(bf16[1536,2048]{1,0:T(8,128)(2,1)} %all-gather.5.cloned.1.call-done, f32[16,3072]{1,0:T(8,128)S(1)} %convert_element_type.82), kind=kOutput, calls=%fused_computation.12 | convolution fusion | flops 100843520 | bytes 6553600 | tf_op jit(solution)/shard_map/dot_general | solution.py:129
  279.6 22.3 %reduce-scatter.11.cloned.1.call-done = bf16[16,512]{1,0:T(8,128)(2,1)} async-done(((bf16[16,2048]{1,0:T(8,128)(2,1)}), bf16[16,512]{1,0:T(8,128)(2,1)}) %reduce-scatter.11.cloned.1.call-update) | async-done | bytes 16400 | tf_op jit(solution)/shard_map/reduce_scatter | solution.py:134
  301.9 1.0 multiply_reduce_fusion.1
  302.9 8.9 %psum.15 = f32[16]{0:T(128)S(1)} all-reduce(f32[16]{0:T(128)S(1)} %get-tuple-element.14), channel_id=1, replica_groups=mesh['ep'=8,'tp'=4] {'tp'}, use_global_device_ids=true, to_apply=%region_13.14 | all-reduce | flops 16 | bytes 128 | tf_op jit(solution)/shard_map/psum | solution.py:139
  311.8 0.7 add_convert_fusion
  (66 shorter events, 2.6 us)
Async XLA Ops:
  7.2 18.1 %copy-start.4 = (s32[16,2]{0,1:T(2,128)S(1)}, s32[16,2]{0,1:T(2,128)}, u32[]{:S(2)}) copy-start(s32[16,2]{0,1:T(2,128)} %param.29) | copy-start | bytes 388
  7.2 18.6 %copy-start.2 = (f32[512]{0:T(512)S(1)}, f32[512]{0:T(512)}, u32[]{:S(2)}) copy-start(f32[512]{0:T(512)} %param.21) | copy-start | bytes 6148
  7.2 47.3 %reduce-scatter.5.cloned.1.call-start = ((), (), s32[]{:S(2)}) async-start(), calls=%async_computation.8 | async-start | bytes 589824 | tf_op jit(solution)/shard_map/reduce_scatter | solution.py:42
  24.5 60.5 %all-gather.3.cloned.1.call-start = ((), (), s32[]{:S(2)}) async-start(), calls=%async_computation.9 | async-start | bytes 2359296 | tf_op jit(solution)/shard_map/all_gather | solution.py:68
  25.2 103.5 %all-reduce.2.cloned.1.call-start = ((), (), s32[]{:S(2)}) async-start(), calls=%async_computation.10 | async-start | bytes 131072 | tf_op jit(solution)/shard_map/psum | solution.py:72
  60.6 2.0 copy-start
  60.6 5.8 %copy-start.5 = (f32[512]{0:T(512)S(1)}, f32[512]{0:T(512)}, u32[]{:S(2)}) copy-start(f32[512]{0:T(512)} %param.22) | copy-start | bytes 6148
  60.6 69.1 %copy-start.1 = (bf16[16,2048]{1,0:T(8,128)(2,1)S(1)}, bf16[16,2048]{1,0:T(8,128)(2,1)}, u32[]{:S(2)}) copy-start(bf16[16,2048]{1,0:T(8,128)(2,1)} %param.19) | copy-start | bytes 196612
  87.6 88.5 %reduce-scatter.7.cloned.1.call-start = ((), (), s32[]{:S(2)}) async-start(), calls=%async_computation.11 | async-start | bytes 327680 | tf_op jit(solution)/shard_map/reduce_scatter | solution.py:101
  148.1 13.9 %copy-start.7 = (bf16[256,1536]{1,0:T(8,128)(2,1)S(1)}, bf16[256,1536]{1,0:T(8,128)(2,1)}, u32[]{:S(2)}) copy-start(bf16[256,1536]{1,0:T(8,128)(2,1)} %param.35) | copy-start | bytes 2359300
  148.1 13.9 %copy-start.8 = (bf16[256,1536]{1,0:T(8,128)(2,1)S(1)}, bf16[256,1536]{1,0:T(8,128)(2,1)}, u32[]{:S(2)}) copy-start(bf16[256,1536]{1,0:T(8,128)(2,1)} %param.34) | copy-start | bytes 2359300
  153.6 10.3 %copy-start.3 = (bf16[2048]{0:T(1024)(128)(2,1)S(1)}, bf16[2048]{0:T(1024)(128)(2,1)}, u32[]{:S(2)}) copy-start(bf16[2048]{0:T(1024)(128)(2,1)} %param.37) | copy-start | bytes 12292
  153.6 10.5 %copy-start.6 = (f32[16,2]{0,1:T(2,128)S(1)}, f32[16,2]{0,1:T(2,128)}, u32[]{:S(2)}) copy-start(f32[16,2]{0,1:T(2,128)} %param.30) | copy-start | bytes 388
  153.7 56.6 %reduce-scatter.9.cloned.1.call-start = ((), (), s32[]{:S(2)}) async-start(), calls=%async_computation.12 | async-start | bytes 884736 | tf_op jit(solution)/shard_map/reduce_scatter | solution.py:121
  163.3 111.8 %all-gather.5.cloned.1.call-start = ((), (), s32[]{:S(2)}) async-start(), calls=%async_computation.13 | async-start | bytes 7077888 | tf_op jit(solution)/shard_map/all_gather | solution.py:131
  176.1 103.5 %all-to-all-start.2 = ((bf16[8,8,512]{2,1,0:T(8,128)(2,1)}), bf16[8,8,512]{2,1,0:T(8,128)(2,1)S(1)}, u32[]{:S(2)}, u32[]{:S(2)}) async-start(bf16[8,8,512]{2,1,0:T(8,128)(2,1)} %reduce-scatter.7.cloned.1.call-done), calls=%async_computation.4 | async-start | bytes 131072 | tf_op jit(solution)/shard_map/all_to_all | solution.py:104
  180.7 121.2 %reduce-scatter.11.cloned.1.call-start = ((), (), s32[]{:S(2)}) async-start(), calls=%async_computation.14 | async-start | bytes 81920 | tf_op jit(solution)/shard_map/reduce_scatter | solution.py:134
Sparse Core Ops, SparseCore 0:
  24.6 29.8 reduce-scatter.4
  56.1 28.8 all-gather.2
  87.9 40.8 all-reduce.1
  153.8 22.2 reduce-scatter.6
  178.2 31.9 reduce-scatter.8
  211.7 63.3 all-gather.4
  279.6 22.2 reduce-scatter.10
where the time goes:
time: 320 us; the launch traced here: 319 us
  waiting for transfers between devices  217 us (68%)
  blocking collectives  43.4 us (14%)
  matrix products  23.7 us (7%)
  between operations  14.4 us (4%)
  other arithmetic  11.5 us (4%)
  starting transfers between devices  4.89 us (2%)
  local copies, waits for them, and re-layouts  4.25 us (1%)
    all_gather x1, waiting for transfers between devices, body(): lax.all_gather(w_dense_down, 'ep', axis=1, tiled=True)  63.9 us
    psum x1, waiting for transfers between devices, body(): mix_out = lax.psum(mix_part.astype(jnp.bfloat16), 'tp')  41.1 us
    reduce_scatter x1, waiting for transfers between devices, body(): lax.psum_scatter(jnp.dot(dense_rows, dense_weights, preferred_element_typ...  29.5 us
    reduce_scatter x1, waiting for transfers between devices, body(): lax.psum_scatter(jnp.dot(mix_rows, in_weights, preferred_element_type=jnp...  28.7 us
    reduce_scatter x1, waiting for transfers between devices, body(): lax.psum_scatter(dense_partial.astype(jnp.bfloat16), 'tp', scatter_dimens...  22.3 us
    all_gather x1, waiting for transfers between devices, body(): lax.all_gather(w_mix_out, 'ep', axis=1, tiled=True)  18.5 us
    all_to_all x1, blocking collectives, body(): lax.all_to_all(outgoing, 'ep', split_axis=0, concat_axis=0, tiled=True)  14.1 us
    all_to_all x1, blocking collectives, body(): lax.all_to_all(normed, 'ep', split_axis=1, concat_axis=0, tiled=True)  12.1 us
  transfers between devices with their start and end apart: 8, of which 7 were waited for; matrix products, arithmetic and copies ran while one was open for 5% of the time, Pallas kernels for 0%

commit v1 on v0

--- a/solution.py
+++ b/solution.py
@@ -69,7 +69,8 @@
         preferred_element_type=jnp.float32,
     ).astype(jnp.bfloat16)
     mix_part = lax.optimization_barrier(mix_part).astype(jnp.float32)
-    mix_out = lax.psum(mix_part.astype(jnp.bfloat16), "tp")
+    a0 = mix_part.astype(jnp.bfloat16)
+    mix_out = lax.all_gather(a0, "tp").sum(axis=0)
     mix_wide = lax.optimization_barrier(mix_out).astype(jnp.float32)
     after_mix = resid + mix_wide * rms_scale(mix_wide) * norm_gains[1]
     ffn_in = (after_mix * rms_scale(after_mix) * norm_gains[2]).astype(jnp.bfloat16)

time: 320 us -> 285 us (0.89)
  waiting for transfers between devices: 217 us -> 177 us
  blocking collectives: 43.4 us -> 50.8 us
    psum x1 -> x0, waiting for transfers between devices: 41.1 us -> none  [body(): mix_out = lax.psum(mix_part.astype(jnp.bfloat16), 'tp')]
    all_gather x0 -> x1, blocking collectives: none -> 8.87 us  [body(): mix_out = lax.all_gather(a0, 'tp').sum(axis=0)]
  transfers between devices with their start and end apart: 8 -> 7, of which waited for: 7 -> 6; matrix products, arithmetic and copies ran while one was open for 5% -> 6% of each run, Pallas kernels for 0% -> 0%
where the time goes in v1:
time: 285 us; the launch traced here: 284 us
  waiting for transfers between devices  177 us (62%)
  blocking collectives  50.8 us (18%)
  matrix products  23.1 us (8%)
  between operations  14.4 us (5%)
  other arithmetic  9.89 us (3%)
  starting transfers between devices  4.83 us (2%)
  local copies, waits for them, and re-layouts  4.25 us (1%)
    all_gather x1, waiting for transfers between devices, body(): lax.all_gather(w_dense_down, 'ep', axis=1, tiled=True)  64.1 us
    reduce_scatter x1, waiting for transfers between devices, body(): lax.psum_scatter(jnp.dot(dense_rows, dense_weights, preferred_element_typ...  29.4 us
    reduce_scatter x1, waiting for transfers between devices, body(): lax.psum_scatter(jnp.dot(mix_rows, in_weights, preferred_element_type=jnp...  28.7 us
    reduce_scatter x1, waiting for transfers between devices, body(): lax.psum_scatter(dense_partial.astype(jnp.bfloat16), 'tp', scatter_dimens...  22.3 us
    all_gather x1, waiting for transfers between devices, body(): lax.all_gather(w_mix_out, 'ep', axis=1, tiled=True)  18.4 us
    all_to_all x1, blocking collectives, body(): lax.all_to_all(outgoing, 'ep', split_axis=0, concat_axis=0, tiled=True)  12.6 us
    reduce_scatter x1, waiting for transfers between devices, body(): lax.psum_scatter(partial_rows.astype(jnp.bfloat16), 'tp', scatter_dimensi...  12.5 us
    all_to_all x1, blocking collectives, body(): lax.all_to_all(normed, 'ep', split_axis=1, concat_axis=0, tiled=True)  12.1 us
  transfers between devices with their start and end apart: 7, of which 6 were waited for; matrix products, arithmetic and copies ran while one was open for 6% of the time, Pallas kernels for 0%

profile of v1, /device:TPU:0, one launch (start us, length us, event | category | flops | bytes accessed | tf_op | source)
XLA Modules:
  0.0 283.9 jit_solution(10849067463388183887)
XLA Ops:
  7.2 0.9 fusion.58
  8.2 1.0 fusion.42
  9.2 0.9 fusion.44
  10.1 12.1 %all_to_all.48 = bf16[16,8,256]{2,0,1:T(8,128)(2,1)S(1)} all-to-all(bf16[16,8,256]{2,0,1:T(8,128)(2,1)S(1)} %bitcast.84), channel_id=1, replica_groups=mesh['ep'=8,'tp'=4] {'ep'}, dimensions={1} | all-to-all | bytes 131072 | tf_op jit(solution)/shard_map/all_to_all | solution.py:41
  22.2 2.3 convolution_convert_fusion.1
  24.5 0.7 all-gather.4.cloned.1.call-update
  25.8 28.7 %reduce-scatter.5.cloned.1.call-done = bf16[16,2048]{1,0:T(8,128)(2,1)} async-done(((bf16[128,2048]{1,0:T(8,128)(2,1)}), bf16[16,2048]{1,0:T(8,128)(2,1)}) %reduce-scatter.5.cloned.1.call-update) | async-done | bytes 65552 | tf_op jit(solution)/shard_map/reduce_scatter | solution.py:42
  54.5 0.8 convert_element_type.72
  55.4 0.7 split.26
  56.2 4.4 %multiply_add_fusion = f32[16,4,128,128]{3,2,1,0:T(8,128)S(1)} fusion(f32[16,4,128,128]{3,2,1,0:T(8,128)} %param.20, f32[16,4,128]{2,1,0:T(4,128)S(1)} %mul.223, f32[16,4,128]{2,1,0:T(4,128)S(1)} %mul.221, f32[16,4,128]{2,1,0:T(4,128)S(1)} %mul.217), kind=kLoop, calls=%fused_computation | loop fusion | flops 3145728 | bytes 8486912 | tf_op jit(solution)/shard_map/add | solution.py:54
  60.6 2.0 copy-done
  62.6 3.7 %fusion.59 = f32[16,4,1,128]{3,2,1,0:T(1,128)S(1)} fusion(f32[16,4,128,1]{2,3,1,0:T(1,128)S(1)} %bitcast.86, f32[16,4,128,128]{3,2,1,0:T(8,128)S(1)} %multiply_add_fusion), kind=kOutput, calls=%fused_computation.92 | convolution fusion | flops 12582912 | bytes 4259840 | tf_op jit(solution)/shard_map/thk,thkv->thv/dot_general | solution.py:58
  66.5 18.4 %all-gather.4.cloned.1.call-done = bf16[512,2048]{1,0:T(8,128)(2,1)} async-done(((bf16[512,256]{1,0:T(8,128)(2,1)}), bf16[512,2048]{1,0:T(8,128)(2,1)}) %all-gather.4.cloned.1.call-update) | async-done | bytes 2097168 | tf_op jit(solution)/shard_map/all_gather | solution.py:68
  84.9 2.0 convolution_convert_fusion.4
  86.9 8.9 %all-gather = bf16[64,2048]{1,0:T(8,128)(2,1)S(1)} all-gather(bf16[16,2048]{1,0:T(8,128)(2,1)S(1)} %convolution_convert_fusion.4), channel_id=2, replica_groups=mesh['ep'=8,'tp'=4] {'tp'}, dimensions={0}, use_global_device_ids=true | all-gather | bytes 327680 | tf_op jit(solution)/shard_map/all_gather | solution.py:73
  95.9 0.2 multiply_reduce_fusion
  96.6 12.6 %all_to_all.49 = bf16[8,8,2048]{2,1,0:T(8,128)(2,1)S(1)} all-to-all(bf16[8,8,2048]{2,1,0:T(8,128)(2,1)S(1)} %fusion.9), channel_id=1, replica_groups=mesh['ep'=8,'tp'=4] {'ep'}, dimensions={0} | all-to-all | bytes 524288 | tf_op jit(solution)/shard_map/all_to_all | solution.py:91
  109.2 2.7 fusion.4
  112.0 5.5 %fusion.6 = bf16[64,2048]{1,0:T(8,128)(2,1)} fusion(bf16[1,896,2048]{2,1,0:T(8,128)(2,1)} %param.33, bf16[1,2048,896]{2,1,0:T(8,128)(2,1)} %param.32, bf16[8,8,2048]{2,1,0:T(8,128)(2,1)S(1)} %all_to_all.49, f32[64,896]{1,0:T(8,128)S(1)} %fusion.4), kind=kOutput, calls=%fused_computation.9 | convolution fusion | flops 470237184 | bytes 8093696 | tf_op jit(solution)/shard_map/dot_general | solution.py:97
  117.6 8.3 %all_to_all.50 = bf16[16,8,256]{2,0,1:T(8,128)(2,1)S(1)} all-to-all(bf16[16,8,256]{2,0,1:T(8,128)(2,1)S(1)} %bitcast.85), channel_id=1, replica_groups=mesh['ep'=8,'tp'=4] {'ep'}, dimensions={1} | all-to-all | bytes 131072 | tf_op jit(solution)/shard_map/all_to_all | solution.py:121
  125.9 1.3 convolution_convert_fusion
  127.2 0.5 all-gather.6.cloned.1.call-update
  128.1 12.5 %reduce-scatter.7.cloned.1.call-done = bf16[8,8,512]{2,1,0:T(8,128)(2,1)} async-done(((bf16[8,8,2048]{2,1,0:T(8,128)(2,1)}), bf16[8,8,512]{2,1,0:T(8,128)(2,1)}) %reduce-scatter.7.cloned.1.call-update) | async-done | bytes 65552 | tf_op jit(solution)/shard_map/reduce_scatter | solution.py:102
  140.6 4.6 %all-to-all-start.2 = ((bf16[8,8,512]{2,1,0:T(8,128)(2,1)}), bf16[8,8,512]{2,1,0:T(8,128)(2,1)S(1)}, u32[]{:S(2)}, u32[]{:S(2)}) async-start(bf16[8,8,512]{2,1,0:T(8,128)(2,1)} %reduce-scatter.7.cloned.1.call-done), calls=%async_computation.4 | async-start | bytes 131072 | tf_op jit(solution)/shard_map/all_to_all | solution.py:105
  145.2 29.4 %reduce-scatter.9.cloned.1.call-done = bf16[16,3072]{1,0:T(8,128)(2,1)} async-done(((bf16[128,3072]{1,0:T(8,128)(2,1)}), bf16[16,3072]{1,0:T(8,128)(2,1)}) %reduce-scatter.9.cloned.1.call-update) | async-done | bytes 98320 | tf_op jit(solution)/shard_map/reduce_scatter | solution.py:122
  174.6 0.9 convert_element_type.84
  175.5 64.1 %all-gather.6.cloned.1.call-done = bf16[1536,2048]{1,0:T(8,128)(2,1)} async-done(((bf16[1536,256]{1,0:T(8,128)(2,1)}), bf16[1536,2048]{1,0:T(8,128)(2,1)}) %all-gather.6.cloned.1.call-update) | async-done | bytes 6291472 | tf_op jit(solution)/shard_map/all_gather | solution.py:132
  239.6 4.3 %convolution_convert_fusion.3 = bf16[16,2048]{1,0:T(8,128)(2,1)} fusion(bf16[1536,2048]{1,0:T(8,128)(2,1)} %all-gather.6.cloned.1.call-done, f32[16,3072]{1,0:T(8,128)S(1)} %convert_element_type.84), kind=kOutput, calls=%fused_computation.12 | convolution fusion | flops 100843520 | bytes 6553600 | tf_op jit(solution)/shard_map/dot_general | solution.py:130
  244.1 22.3 %reduce-scatter.11.cloned.1.call-done = bf16[16,512]{1,0:T(8,128)(2,1)} async-done(((bf16[16,2048]{1,0:T(8,128)(2,1)}), bf16[16,512]{1,0:T(8,128)(2,1)}) %reduce-scatter.11.cloned.1.call-update) | async-done | bytes 16400 | tf_op jit(solution)/shard_map/reduce_scatter | solution.py:135
  266.4 1.0 multiply_reduce_fusion.1
  267.4 8.9 %psum.7 = f32[16]{0:T(128)S(1)} all-reduce(f32[16]{0:T(128)S(1)} %get-tuple-element.14), channel_id=1, replica_groups=mesh['ep'=8,'tp'=4] {'tp'}, use_global_device_ids=true, to_apply=%region_13.14 | all-reduce | flops 16 | bytes 128 | tf_op jit(solution)/shard_map/psum | solution.py:140
  276.3 0.7 add_convert_fusion
  (65 shorter events, 2.2 us)
Async XLA Ops:
  7.2 18.1 %copy-start.4 = (s32[16,2]{0,1:T(2,128)S(1)}, s32[16,2]{0,1:T(2,128)}, u32[]{:S(2)}) copy-start(s32[16,2]{0,1:T(2,128)} %param.29) | copy-start | bytes 388
  7.2 18.6 %copy-start.2 = (f32[512]{0:T(512)S(1)}, f32[512]{0:T(512)}, u32[]{:S(2)}) copy-start(f32[512]{0:T(512)} %param.21) | copy-start | bytes 6148
  7.2 47.3 %reduce-scatter.5.cloned.1.call-start = ((), (), s32[]{:S(2)}) async-start(), calls=%async_computation.8 | async-start | bytes 589824 | tf_op jit(solution)/shard_map/reduce_scatter | solution.py:42
  24.5 60.4 %all-gather.4.cloned.1.call-start = ((), (), s32[]{:S(2)}) async-start(), calls=%async_computation.9 | async-start | bytes 2359296 | tf_op jit(solution)/shard_map/all_gather | solution.py:68
  25.2 115.3 %reduce-scatter.7.cloned.1.call-start = ((), (), s32[]{:S(2)}) async-start(), calls=%async_computation.10 | async-start | bytes 327680 | tf_op jit(solution)/shard_map/reduce_scatter | solution.py:102
  60.6 2.0 copy-start
  60.6 5.8 %copy-start.5 = (f32[512]{0:T(512)S(1)}, f32[512]{0:T(512)}, u32[]{:S(2)}) copy-start(f32[512]{0:T(512)} %param.22) | copy-start | bytes 6148
  60.6 35.3 %copy-start.1 = (bf16[16,2048]{1,0:T(8,128)(2,1)S(1)}, bf16[16,2048]{1,0:T(8,128)(2,1)}, u32[]{:S(2)}) copy-start(bf16[16,2048]{1,0:T(8,128)(2,1)} %param.19) | copy-start | bytes 196612
  111.9 13.9 %copy-start.7 = (bf16[256,1536]{1,0:T(8,128)(2,1)S(1)}, bf16[256,1536]{1,0:T(8,128)(2,1)}, u32[]{:S(2)}) copy-start(bf16[256,1536]{1,0:T(8,128)(2,1)} %param.35) | copy-start | bytes 2359300
  112.0 13.9 %copy-start.8 = (bf16[256,1536]{1,0:T(8,128)(2,1)S(1)}, bf16[256,1536]{1,0:T(8,128)(2,1)}, u32[]{:S(2)}) copy-start(bf16[256,1536]{1,0:T(8,128)(2,1)} %param.34) | copy-start | bytes 2359300
  117.5 10.4 %copy-start.3 = (bf16[2048]{0:T(1024)(128)(2,1)S(1)}, bf16[2048]{0:T(1024)(128)(2,1)}, u32[]{:S(2)}) copy-start(bf16[2048]{0:T(1024)(128)(2,1)} %param.37) | copy-start | bytes 12292
  117.5 10.5 %copy-start.6 = (f32[16,2]{0,1:T(2,128)S(1)}, f32[16,2]{0,1:T(2,128)}, u32[]{:S(2)}) copy-start(f32[16,2]{0,1:T(2,128)} %param.30) | copy-start | bytes 388
  117.5 57.1 %reduce-scatter.9.cloned.1.call-start = ((), (), s32[]{:S(2)}) async-start(), calls=%async_computation.11 | async-start | bytes 884736 | tf_op jit(solution)/shard_map/reduce_scatter | solution.py:122
  127.2 112.4 %all-gather.6.cloned.1.call-start = ((), (), s32[]{:S(2)}) async-start(), calls=%async_computation.12 | async-start | bytes 7077888 | tf_op jit(solution)/shard_map/all_gather | solution.py:132
  140.6 103.5 %all-to-all-start.2 = ((bf16[8,8,512]{2,1,0:T(8,128)(2,1)}), bf16[8,8,512]{2,1,0:T(8,128)(2,1)S(1)}, u32[]{:S(2)}, u32[]{:S(2)}) async-start(bf16[8,8,512]{2,1,0:T(8,128)(2,1)} %reduce-scatter.7.cloned.1.call-done), calls=%async_computation.4 | async-start | bytes 131072 | tf_op jit(solution)/shard_map/all_to_all | solution.py:105
  145.2 121.2 %reduce-scatter.11.cloned.1.call-start = ((), (), s32[]{:S(2)}) async-start(), calls=%async_computation.13 | async-start | bytes 81920 | tf_op jit(solution)/shard_map/reduce_scatter | solution.py:135
Sparse Core Ops, SparseCore 0:
  24.6 29.8 reduce-scatter.4
  56.1 28.7 all-gather.3
  117.6 22.8 reduce-scatter.6
  142.7 31.8 reduce-scatter.8
  176.0 63.5 all-gather.5
  244.1 22.2 reduce-scatter.10
